TPU v7x, 32 devices: a whole 2x2x4 slice. The times are simulated.
32 devices in a mesh: sp: 8 (over z, x), tp: 4 (over y, core).
Axes of the slice: x: 2, y: 2, z: 4, core: 2. Of those that a mesh axis runs over, the one named last changes fastest.
Arguments:
- resid: bfloat16 [2048, 2048], P('sp'), may hold values from -6 to 6
- query_one: bfloat16 [2048, 1024], P('sp', 'tp'), may hold values from -400 to 400
- query_two: bfloat16 [2048, 1024], P('sp', 'tp'), may hold values from -400 to 400
- key_one: bfloat16 [2048, 1024], P('sp', 'tp'), may hold values from -8 to 8
- key_two: bfloat16 [2048, 1024], P('sp', 'tp'), may hold values from -8 to 8
- values: bfloat16 [2048, 2048], P('sp', 'tp'), may hold values from -6 to 6
- documents: int32 [2048], P('sp'), may hold values from 0 to 1, never falling along the last dimension, each value on 1 to 1280 neighbouring positions
- mix_lambda: float32 [16], P('tp'), may hold values from 0.3 to 0.8
- head_gain: float32 [128], replicated, may hold values from 0.1 to 1.9
- out_weight: bfloat16 [2048, 2048], P('tp'), may hold values from -0.125 to 0.125
- ffn_gain: float32 [2048], replicated, may hold values from 0.1 to 1.9
- routes: int32 [2048, 4], P('sp'), may hold values from 0 to 31, all different within a row; in each aligned block of 256 rows (0 to 255, 256 to 511, ...) at most 64 rows name the same one
- route_weight: float32 [2048, 4], P('sp'), may hold values from 0.2 to 0.9
- expert_gate: bfloat16 [32, 2048, 512], P(('sp', 'tp')), may hold values from -0.125 to 0.125
- expert_up: bfloat16 [32, 2048, 512], P(('sp', 'tp')), may hold values from -0.125 to 0.125
- expert_down: bfloat16 [32, 512, 2048], P(('sp', 'tp')), may hold values from -0.25 to 0.25
- shared_gate: bfloat16 [2048, 512], P(None, 'tp'), may hold values from -0.125 to 0.125
- shared_up: bfloat16 [2048, 512], P(None, 'tp'), may hold values from -0.125 to 0.125
- shared_down: bfloat16 [512, 2048], P('tp'), may hold values from -0.25 to 0.25
Outputs:
- layer_out: bfloat16 [2048, 2048], P(('sp', 'tp'))
Inputs may be any that keep to these rules, and one draw needn't show every extreme that they name: `documents`: document numbers never fall along the positions; each document has 1 to 1280 positions and one has exactly 1280. `routes`: A row names 4 different experts. In each aligned block of 256 rows no expert is named by more than 64 rows, a bound that some block reaches.
All inputs are finite; a program needn't handle non-finite values.
Results may differ from a plain program's by a relative error of at most 0.018.
Values may be sent and summed in bfloat16 or wider, within the bound.
A program may use at most 128 MiB of HBM per device.

v0:
```python
import jax
import jax.numpy as jnp
from jax import lax
from jax.sharding import PartitionSpec as P

NEG_FILL = -1e30
HEAD_SCALE = 0.8


def rms_scale(values_in, eps_value):
    return lax.rsqrt(jnp.mean(values_in * values_in, axis=-1, keepdims=True) + eps_value)


def local(
    resid,
    query_one,
    query_two,
    key_one,
    key_two,
    values,
    documents,
    mix_lambda,
    head_gain,
    out_weight,
    ffn_gain,
    routes,
    route_weight,
    expert_gate,
    expert_up,
    expert_down,
    shared_gate,
    shared_up,
    shared_down,
):
    tok_rows = query_one.shape[0]
    head_count = mix_lambda.shape[0]
    head_width = query_one.shape[1] // head_count
    value_width = values.shape[1] // head_count
    model_width = resid.shape[1]
    score_scale = head_width ** (-0.5)
    seq_size = lax.axis_size("sp")
    tp_size = lax.axis_size("tp")
    query_pos = lax.axis_index("sp") * tok_rows + jnp.arange(tok_rows, dtype=jnp.int32)
    query_first = query_one.reshape(tok_rows, head_count, head_width)
    query_second = query_two.reshape(tok_rows, head_count, head_width)
    lambda_col = mix_lambda[:, None, None]
    first_doc = documents[0]
    last_pos = query_pos[tok_rows - 1]

    def masks(key_docs):
        key_pos = jnp.arange(key_docs.shape[0], dtype=jnp.int32)
        return (
            (key_pos[None, :] <= query_pos[:, None]) & (key_docs[None, :] == documents[:, None])
        )[None]

    def needed(key_docs, offset):
        return (offset <= last_pos) & (jnp.max(key_docs) >= first_doc)

    def scores(query_block, key_block):
        keyed = key_block.reshape(key_block.shape[0], head_count, head_width)
        return (
            jnp.einsum("qhd,khd->hqk", query_block, keyed, preferred_element_type=jnp.float32)
            * score_scale
        )

    empty_max = jnp.full((head_count, tok_rows), NEG_FILL, jnp.float32)
    empty_sum = jnp.zeros((head_count, tok_rows), jnp.float32)
    stats_init = ((empty_max, empty_sum), (empty_max, empty_sum))
    value_init = jnp.zeros((head_count, tok_rows, value_width), jnp.float32)
    key_first = lax.all_gather(key_one, "sp", axis=0, tiled=True)
    key_second = lax.all_gather(key_two, "sp", axis=0, tiled=True)
    key_docs = lax.all_gather(documents, "sp", axis=0, tiled=True)

    def stats_update(current):
        allowed = masks(key_docs)
        result = []
        for query_block, key_block, (top_now, sum_now) in (
            (query_first, key_first, current[0]),
            (query_second, key_second, current[1]),
        ):
            masked = jnp.where(allowed, scores(query_block, key_block), NEG_FILL)
            top_next = jnp.maximum(top_now, jnp.max(masked, axis=-1))
            fresh = jnp.where(allowed, jnp.exp(masked - top_next[:, :, None]), 0.0)
            result.append((top_next, jnp.sum(fresh, axis=-1)))
        return tuple(result)

    def stats_keep(current):
        return current

    soft_stats = lax.cond(needed(key_docs, jnp.int32(0)), stats_update, stats_keep, stats_init)
    apply_key_first = lax.all_gather(key_one, "sp", axis=0, tiled=True)
    apply_key_second = lax.all_gather(key_two, "sp", axis=0, tiled=True)
    value_block = lax.all_gather(values, "sp", axis=0, tiled=True)
    apply_key_docs = lax.all_gather(documents, "sp", axis=0, tiled=True)

    def apply_update(current):
        allowed = masks(apply_key_docs)
        probs = []
        for query_block, key_block, (top_all, sum_all) in (
            (query_first, apply_key_first, soft_stats[0]),
            (query_second, apply_key_second, soft_stats[1]),
        ):
            raw = scores(query_block, key_block)
            probs.append(
                jnp.where(allowed, jnp.exp(raw - top_all[:, :, None]), 0.0) / sum_all[:, :, None]
            )
        weights = (probs[0] - lambda_col * probs[1]).astype(jnp.bfloat16)
        valued = value_block.reshape(value_block.shape[0], head_count, value_width)
        return current + jnp.einsum(
            "hqk,khv->hqv", weights, valued, preferred_element_type=jnp.float32
        )

    def apply_keep(current):
        return current

    head_out = lax.cond(needed(apply_key_docs, jnp.int32(0)), apply_update, apply_keep, value_init)
    normed_heads = (head_out * rms_scale(head_out, 1e-05) * head_gain * HEAD_SCALE).astype(
        jnp.bfloat16
    )
    attn_rows = normed_heads.transpose(1, 0, 2).reshape(tok_rows, head_count * value_width)
    share_rows = tok_rows // tp_size
    own_start = lax.axis_index("tp") * share_rows
    proj_term = jnp.dot(attn_rows, out_weight, preferred_element_type=jnp.float32)
    projected = lax.psum(proj_term.astype(jnp.bfloat16), "tp").astype(jnp.float32)
    mixed_all = resid.astype(jnp.float32) + projected
    normed_all = (mixed_all * rms_scale(mixed_all, 1e-06) * ffn_gain).astype(jnp.bfloat16)
    mixed_own = lax.dynamic_slice_in_dim(mixed_all, own_start, share_rows, 0)
    route_slots = routes.shape[1]
    capacity = max(2, 2 * tok_rows * route_slots // (seq_size * tp_size))
    assign_total = tok_rows * route_slots
    flat_expert = routes.reshape(assign_total)
    flat_weight = route_weight.reshape(assign_total)
    assign_token = jnp.arange(assign_total, dtype=jnp.int32) // route_slots
    is_mine = flat_expert % tp_size == lax.axis_index("tp")
    target = flat_expert // tp_size
    one_hot = (
        (target[:, None] == jnp.arange(seq_size, dtype=jnp.int32)[None, :]) & is_mine[:, None]
    ).astype(jnp.int32)
    slot_rank = jnp.sum(jnp.cumsum(one_hot, axis=0) * one_hot, axis=1) - 1
    slot_id = jnp.where(is_mine, target * capacity + slot_rank, -1)
    slot_total = seq_size * capacity
    matches = slot_id[None, :] == jnp.arange(slot_total, dtype=jnp.int32)[:, None]
    slot_token = jnp.sum(jnp.where(matches, assign_token[None, :], 0), axis=1)
    slot_live = jnp.any(matches, axis=1)
    outgoing = jnp.where(
        slot_live[:, None], normed_all[slot_token], jnp.zeros((), jnp.bfloat16)
    ).reshape(seq_size, capacity, model_width)
    arrived = lax.all_to_all(outgoing, "sp", split_axis=0, concat_axis=0, tiled=True)
    item_count = arrived.shape[1]
    flat_rows = arrived.reshape(seq_size * item_count, model_width)
    gate_part = jnp.dot(flat_rows, expert_gate[0], preferred_element_type=jnp.float32)
    up_part = jnp.dot(flat_rows, expert_up[0], preferred_element_type=jnp.float32)
    hidden = (jax.nn.silu(gate_part) * up_part).astype(jnp.bfloat16)
    result = jnp.dot(hidden, expert_down[0], preferred_element_type=jnp.float32).astype(
        jnp.bfloat16
    )
    returned = lax.all_to_all(
        result.reshape(seq_size, item_count, model_width),
        "sp",
        split_axis=0,
        concat_axis=0,
        tiled=True,
    )
    returned_flat = returned.reshape(slot_total, model_width)
    picked = returned_flat[jnp.maximum(slot_id, 0)].astype(jnp.float32)
    picked_weight = jnp.where(is_mine, flat_weight, 0.0)
    routed = jnp.sum(
        (picked * picked_weight[:, None]).reshape(tok_rows, route_slots, model_width), axis=1
    )
    shared_act = (
        jax.nn.silu(jnp.dot(normed_all, shared_gate, preferred_element_type=jnp.float32))
        * jnp.dot(normed_all, shared_up, preferred_element_type=jnp.float32)
    ).astype(jnp.bfloat16)
    shared_out = jnp.dot(shared_act, shared_down, preferred_element_type=jnp.float32)
    ffn_own = lax.psum_scatter(
        (routed + shared_out).astype(jnp.bfloat16), "tp", scatter_dimension=0, tiled=True
    ).astype(jnp.float32)
    return (mixed_own + ffn_own).astype(jnp.bfloat16)


def solution(mesh):
    placed = (
        P("sp", None),
        P("sp", "tp"),
        P("sp", "tp"),
        P("sp", "tp"),
        P("sp", "tp"),
        P("sp", "tp"),
        P("sp"),
        P("tp"),
        P(),
        P("tp", None),
        P(),
        P("sp", None),
        P("sp", None),
        P(("sp", "tp"), None, None),
        P(("sp", "tp"), None, None),
        P(("sp", "tp"), None, None),
        P(None, "tp"),
        P(None, "tp"),
        P("tp", None),
    )
    return jax.shard_map(
        local, mesh=mesh, in_specs=placed, out_specs=P(("sp", "tp"), None), check_vma=False
    )
```

profile of v0, /device:TPU:0, one launch (start us, length us, event | category | flops | bytes accessed | tf_op | source)
XLA Modules:
  0.0 388.5 jit_solution(5894218725486632129)
XLA Ops:
  6.5 1.8 copy.47
  8.4 1.7 copy.49
  10.2 1.8 copy.51
  12.0 0.8 copy.52
  13.1 1.0 copy.48
  14.2 0.6 slice.12
  14.8 0.5 slice.13
  15.9 22.3 %all-gather = s32[8,1,256]{2,1,0:T(1,128)S(1)} all-gather(s32[1,1,256]{2,1,0:T(1,128)S(1)} %bitcast.92), channel_id=1, replica_groups=mesh['sp'=8,'tp'=4] {'sp'}, dimensions={0}, use_global_device_ids=true | all-gather | bytes 9216 | tf_op jit(solution)/shard_map/all_gather | solution.py:94
  38.2 0.6 reduce_max.29
  40.0 2.3 reduce-window.6
  42.3 0.3 slice_reduce_fusion
  42.6 0.2 reduce-window.9
  42.9 8.6 %all-gather.5.cloned.1.call-done = bf16[2048,256]{0,1:T(8,128)(2,1)} async-done(((bf16[256,256]{0,1:T(8,128)(2,1)}), bf16[2048,256]{0,1:T(8,128)(2,1)}) %all-gather.5.cloned.1.call-update) | async-done | bytes 1048592 | tf_op jit(solution)/shard_map/all_gather | solution.py:91
  51.6 40.5 %all-gather.7.cloned.1.call-done = bf16[2048,256]{0,1:T(8,128)(2,1)} async-done(((bf16[256,256]{0,1:T(8,128)(2,1)}), bf16[2048,256]{0,1:T(8,128)(2,1)}) %all-gather.7.cloned.1.call-update) | async-done | bytes 1048592 | tf_op jit(solution)/shard_map/all_gather | solution.py:71
  92.0 12.4 %conditional.2 = (f32[4,256]{1,0:T(4,128)}, f32[4,256]{1,0:T(4,128)S(1)}, f32[4,256]{1,0:T(4,128)}, f32[4,256]{1,0:T(4,128)S(1)}) conditional(s32[]{:T(128)} %convert_element_type.53, () %tuple.24, (s32[256]{0:T(256)S(1)}, s32[2048]{0:T(1024)S(1)}, s32[256]{0:T(256)S(1)}, bf16[2048,256]{0,1:T(8,128)(2,1)}, bf16[256,4,64]{0,2,1:T(8,128)(2,1)S(1)}, ...), branch_computations={%region_1.0_spmd, %region_2.7_spmd} | conditional | flops 571996160 | bytes 50120764 | solution.py:90
  92.0 2.6 fusion.55
  94.6 0.5 fusion.2
  95.2 3.1 fusion.1
  98.3 0.6 broadcast_maximum_fusion
  98.9 5.5 %select_reduce_fusion = (f32[4,256]{1,0:T(4,128)S(1)}, f32[4,256]{1,0:T(4,128)S(1)}) fusion(f32[4,256,2048]{2,1,0:T(8,128)S(1)} %get-tuple-element.106, f32[4,256]{1,0:T(4,128)} %get-tuple-element.122, pred[256,2048]{1,0:T(8,128)(4,1)S(1)} %fusion.2, f32[4,256]{1,0:T(4,128)} %get-tuple-element.120, f32[4,256,2048]{2,1,0:T(8,128)S(1)} %fusion.55), kind=kLoop, calls=%fused_computation.2 | loop fusion | flops 20969472 | bytes 17317888 | tf_op jit(solution)/shard_map/cond/branch_1_fun/reduce_sum | solution.py:84
  104.4 39.0 %all-gather.9.cloned.1.call-done = bf16[2048,512]{0,1:T(8,128)(2,1)} async-done(((bf16[256,512]{0,1:T(8,128)(2,1)}), bf16[2048,512]{0,1:T(8,128)(2,1)}) %all-gather.9.cloned.1.call-update) | async-done | bytes 2097168 | tf_op jit(solution)/shard_map/all_gather | solution.py:93
  143.5 16.7 %conditional.3 = (f32[4,256,128]{1,2,0:T(8,128)S(1)}, f32[4,256,1]{1,0,2:T(4,128)S(1)}) conditional(s32[]{:T(128)} %convert_element_type.53, () %tuple.23, (s32[256]{0:T(256)S(1)}, s32[2048]{0:T(1024)S(1)}, s32[256]{0:T(256)S(1)}, bf16[2048,256]{0,1:T(8,128)(2,1)}, bf16[256,4,64]{0,2,1:T(8,128)(2,1)S(1)}, /*index=5*/f32[4,256]{1,0:T(4,128)}, ...), branch_computations={%region_7.8_spmd, %region_8.0_spmd} | conditional | flops 1098644480 | bytes 22837280 | solution.py:116
  143.5 5.7 %fusion.56 = f32[4,256,2048]{2,1,0:T(8,128)} fusion(bf16[256,4,64]{0,2,1:T(8,128)(2,1)S(1)} %get-tuple-element.58, bf16[2048,4,64]{0,2,1:T(8,128)(2,1)} %bitcast.75), kind=kOutput, calls=%fused_computation.113 | convolution fusion | flops 268435456 | bytes 9568256 | tf_op jit(solution)/shard_map/cond/branch_1_fun/qhd,khd->hqk/dot_general | solution.py:62
  149.2 1.4 fusion.9
  150.6 9.6 %multiply_reduce_fusion = (f32[4,256]{1,0:T(4,128)S(1)}, f32[4,256,128]{1,2,0:T(8,128)S(1)}) fusion(bf16[2048,4,128]{0,2,1:T(8,128)(2,1)} %bitcast.95, f32[4,256,2048]{2,1,0:T(8,128)} %fusion.56, bf16[256,4,64]{0,2,1:T(8,128)(2,1)S(1)} %get-tuple-element.63, bf16[2048,4,64]{0,2,1:T(8,128)(2,1)} %bitcast.82, f32[4,256]{1,0:T(4,128)S(1)} %get-tuple-element.66, ...), kind=kOutput, calls=%fused_computation.21 | convolution fusion | flops 828636160 | bytes 12734480 | tf_op jit(solution)/shard_map/cond/branch_1_fun/hqk,khv->hqv/dot_general | solution.py:109
  160.4 3.4 convolution_convert_fusion.1
  163.9 0.3 fusion.18
  164.3 0.3 select_reduce_fusion.2
  164.6 33.9 %all-reduce.2.cloned.1.call-done = bf16[256,2048]{1,0:T(8,128)(2,1)} async-done(((bf16[256,2048]{1,0:T(8,128)(2,1)}), bf16[256,2048]{1,0:T(8,128)(2,1)}) %all-reduce.2.cloned.1.call-update) | async-done | bytes 1048592 | tf_op jit(solution)/shard_map/psum | solution.py:124
  198.5 3.1 convert_add_fusion
  201.6 0.6 multiply_convert_fusion
  202.2 3.3 gather_fusion
  205.5 1.8 broadcast_select_fusion
  207.3 53.2 %all_to_all.10 = bf16[8,64,2048]{2,1,0:T(8,128)(2,1)S(1)} all-to-all(bf16[8,64,2048]{2,1,0:T(8,128)(2,1)S(1)} %broadcast_select_fusion), channel_id=1, replica_groups=mesh['sp'=8,'tp'=4] {'sp'}, dimensions={0} | all-to-all | bytes 4194304 | tf_op jit(solution)/shard_map/all_to_all | solution.py:148
  260.5 1.3 copy-done.4
  261.8 2.2 fusion.16
  264.1 6.3 %convolution_convert_fusion = bf16[512,2048]{1,0:T(8,128)(2,1)} fusion(bf16[1,512,2048]{2,1,0:T(8,128)(2,1)S(1)} %copy-done, bf16[512,2048]{1,0:T(8,128)(2,1)} %bitcast.78, bf16[1,2048,512]{2,1,0:T(8,128)(2,1)} %param.37, f32[512,512]{1,0:T(8,128)} %fusion.16), kind=kOutput, calls=%fused_computation.25 | convolution fusion | flops 2150105088 | bytes 9437184 | tf_op jit(solution)/shard_map/dot_general | solution.py:154
  270.3 4.5 %all-to-all-start.1 = ((bf16[8,64,2048]{2,1,0:T(8,128)(2,1)}), bf16[8,64,2048]{2,1,0:T(8,128)(2,1)}, u32[]{:S(2)}, u32[]{:S(2)}) async-start(bf16[8,64,2048]{2,1,0:T(8,128)(2,1)} %bitcast.76), calls=%async_computation.1 | async-start | bytes 4194304 | tf_op jit(solution)/shard_map/all_to_all | solution.py:157
  274.9 0.1 reshape.440
  275.1 0.1 copy.55
  275.3 1.5 fusion.57
  276.7 45.4 %all-to-all-done.1 = bf16[8,64,2048]{2,1,0:T(8,128)(2,1)} async-done(((bf16[8,64,2048]{2,1,0:T(8,128)(2,1)}), bf16[8,64,2048]{2,1,0:T(8,128)(2,1)}, u32[]{:S(2)}, u32[]{:S(2)}) %all-to-all-start.1) | async-done | bytes 2097184 | tf_op jit(solution)/shard_map/all_to_all | solution.py:157
  322.1 10.7 %gather_fusion.1 = bf16[1024,2048]{1,0:T(8,128)(2,1)} fusion(bf16[512,2048]{1,0:T(8,128)(2,1)} %bitcast.24, s32[1024]{0:T(1024)S(1)} %broadcast_clamp_fusion), kind=kCustom, calls=%fused_computation.1 | custom fusion | bytes 8392704 | tf_op jit(solution)/shard_map/gather | solution.py:165
  332.8 8.3 %reshape.441 = f32[256,4,2048]{2,1,0:T(4,128)} reshape(bf16[1024,2048]{1,0:T(8,128)(2,1)} %gather_fusion.1) | data formatting | bytes 12582912 | tf_op jit(solution)/shard_map/convert_element_type | solution.py:165
  341.1 11.4 %multiply_reduce_fusion.1 = f32[256,2048]{1,0:T(8,128)} fusion(f32[256,4,2048]{2,1,0:T(4,128)} %reshape.441, f32[256,4]{1,0:T(8,128)S(1)} %copy.55), kind=kLoop, calls=%fused_computation.24 | loop fusion | flops 3670016 | bytes 10489856 | tf_op jit(solution)/shard_map/reduce_sum | solution.py:167
  352.5 3.7 fusion.12
  356.2 23.9 %reduce-scatter.2.cloned.1.call-done = bf16[64,2048]{1,0:T(8,128)(2,1)} async-done(((bf16[256,2048]{1,0:T(8,128)(2,1)}), bf16[64,2048]{1,0:T(8,128)(2,1)}) %reduce-scatter.2.cloned.1.call-update) | async-done | bytes 262160 | tf_op jit(solution)/shard_map/reduce_scatter | solution.py:175
  380.1 1.9 add_convert_fusion
  (58 shorter events, 1.1 us)
Async XLA Ops:
  6.5 257.5 %copy-start = (bf16[1,512,2048]{2,1,0:T(8,128)(2,1)S(1)}, bf16[1,512,2048]{2,1,0:T(8,128)(2,1)}, u32[]{:S(2)}) copy-start(bf16[1,512,2048]{2,1,0:T(8,128)(2,1)} %param.38) | copy-start | bytes 6291460
  6.5 7.6 %copy-start.6 = (bf16[256,256]{1,0:T(8,128)(2,1)S(1)}, bf16[256,256]{1,0:T(8,128)(2,1)}, u32[]{:S(2)}) copy-start(bf16[256,256]{1,0:T(8,128)(2,1)} %param.25) | copy-start | bytes 393220
  6.5 8.3 %copy-start.8 = (s32[256]{0:T(256)S(1)}, s32[256]{0:T(256)}, u32[]{:S(2)}) copy-start(s32[256]{0:T(256)} %param.29) | copy-start | bytes 3076
  6.5 45.0 %all-gather.5.cloned.1.call-start = ((), (), s32[]{:S(2)}) async-start(), calls=%async_computation.3 | async-start | bytes 1179648 | tf_op jit(solution)/shard_map/all_gather | solution.py:91
  8.4 83.7 %all-gather.7.cloned.1.call-start = ((), (), s32[]{:S(2)}) async-start(), calls=%async_computation.4 | async-start | bytes 1179648 | tf_op jit(solution)/shard_map/all_gather | solution.py:71
  10.1 133.4 %all-gather.9.cloned.1.call-start = ((), (), s32[]{:S(2)}) async-start(), calls=%async_computation.5 | async-start | bytes 2359296 | tf_op jit(solution)/shard_map/all_gather | solution.py:93
  12.0 186.5 %all-reduce.2.cloned.1.call-start = ((), (), s32[]{:S(2)}) async-start(), calls=%async_computation.6 | async-start | bytes 2097152 | tf_op jit(solution)/shard_map/psum | solution.py:124
  92.0 51.5 %copy-start.13 = (f32[4]{0:T(128)S(1)}, f32[4]{0:T(128)}, u32[]{:S(2)}) copy-start(f32[4]{0:T(128)} %param.30) | copy-start | bytes 52
  92.0 3.2 copy-start.5
  143.5 16.8 %copy-start.11 = (f32[128]{0:T(128)S(1)}, f32[128]{0:T(128)}, u32[]{:S(2)}) copy-start(f32[128]{0:T(128)} %param.31) | copy-start | bytes 1540
  160.4 38.1 %copy-start.1 = (bf16[256,2048]{1,0:T(8,128)(2,1)S(1)}, bf16[256,2048]{1,0:T(8,128)(2,1)}, u32[]{:S(2)}) copy-start(bf16[256,2048]{1,0:T(8,128)(2,1)} %param.23) | copy-start | bytes 3145732
  164.6 37.0 %copy-start.9 = (f32[2048]{0:T(1024)S(1)}, f32[2048]{0:T(1024)}, u32[]{:S(2)}) copy-start(f32[2048]{0:T(1024)} %param.33) | copy-start | bytes 24580
  198.5 3.1 copy-start.2
  198.5 3.1 copy-start.3
  207.3 54.5 %copy-start.12 = (bf16[1,2048,512]{2,1,0:T(8,128)(2,1)S(1)}, bf16[1,2048,512]{2,1,0:T(8,128)(2,1)}, u32[]{:S(2)}) copy-start(bf16[1,2048,512]{2,1,0:T(8,128)(2,1)} %param.36) | copy-start | bytes 6291460
  260.5 1.3 copy-start.4
  270.3 4.7 %copy-start.7 = (s32[256,4]{0,1:T(4,128)S(1)}, s32[256,4]{0,1:T(4,128)}, u32[]{:S(2)}) copy-start(s32[256,4]{0,1:T(4,128)} %param.34) | copy-start | bytes 12292
  270.3 4.7 %copy-start.10 = (f32[256,4]{0,1:T(4,128)S(1)}, f32[256,4]{0,1:T(4,128)}, u32[]{:S(2)}) copy-start(f32[256,4]{0,1:T(4,128)} %param.35) | copy-start | bytes 12292
  270.3 51.7 %all-to-all-start.1 = ((bf16[8,64,2048]{2,1,0:T(8,128)(2,1)}), bf16[8,64,2048]{2,1,0:T(8,128)(2,1)}, u32[]{:S(2)}, u32[]{:S(2)}) async-start(bf16[8,64,2048]{2,1,0:T(8,128)(2,1)} %bitcast.76), calls=%async_computation.1 | async-start | bytes 4194304 | tf_op jit(solution)/shard_map/all_to_all | solution.py:157
  274.8 105.3 %reduce-scatter.2.cloned.1.call-start = ((), (), s32[]{:S(2)}) async-start(), calls=%async_computation.7 | async-start | bytes 1310720 | tf_op jit(solution)/shard_map/reduce_scatter | solution.py:175
Sparse Core Ops, SparseCore 0:
  9.4 42.1 all-gather.4
  53.6 38.3 all-gather.6
  94.1 49.3 all-gather.8
  164.0 34.4 all-reduce.1
  356.3 23.7 reduce-scatter.1
where the time goes:
time: 389 us
  waiting for transfers between devices  191 us (49%)
  blocking collectives  75.5 us (19%)
  matrix products  38.2 us (10%)
  local copies, waits for them, and re-layouts  32.8 us (8%)
  other arithmetic  30.8 us (8%)
  between operations  15.1 us (4%)
  starting transfers between devices  4.67 us (1%)
    all_to_all x1, blocking collectives, local(): lax.all_to_all(outgoing, 'sp', split_axis=0, concat_axis=0, tiled=True)  53.2 us
    all_to_all x1, waiting for transfers between devices, local(): lax.all_to_all(result.reshape(seq_size, item_count, model_width), 'sp', s...  45.4 us
    all_gather x1, waiting for transfers between devices, local(): key_second = lax.all_gather(key_two, 'sp', axis=0, tiled=True)  40.5 us
    all_gather x1, waiting for transfers between devices, local(): value_block = lax.all_gather(values, 'sp', axis=0, tiled=True)  39 us
    psum x1, waiting for transfers between devices, local(): lax.psum(proj_term.astype(jnp.bfloat16), 'tp').astype(jnp.float32)  33.9 us
    reduce_scatter x1, waiting for transfers between devices, local(): lax.psum_scatter((routed + shared_out).astype(jnp.bfloat16), 'tp', scatte...  23.9 us
    all_gather x1, blocking collectives, local(): apply_key_docs = lax.all_gather(documents, 'sp', axis=0, tiled=True)  22.3 us
    dot_general x3, matrix products, scores(): jnp.einsum('qhd,khd->hqk', query_block, keyed, preferred_element_type=jnp...  11.5 us
  transfers between devices with their start and end apart: 6, of which 6 were waited for; matrix products, arithmetic and copies ran while one was open for 6% of the time, Pallas kernels for 0%

commit v1 on v0

--- a/solution.py
+++ b/solution.py
@@ -5,6 +5,19 @@
 
 NEG_FILL = -1e30
 HEAD_SCALE = 0.8
+
+
+def collect(array, axis, dim):
+    ways = lax.axis_size(axis)
+    up = [(d, (d + 1) % ways) for d in range(ways)]
+    down = [(d, (d - 1) % ways) for d in range(ways)]
+    earlier, later = ([array], [array])
+    for _ in range(ways // 2):
+        earlier.append(lax.ppermute(earlier[-1], axis, up))
+    for _ in range((ways - 1) // 2):
+        later.append(lax.ppermute(later[-1], axis, down))
+    line = jnp.concatenate([*earlier[::-1], *later[1:]], axis=dim)
+    return jnp.roll(line, (lax.axis_index(axis) - ways // 2) * array.shape[dim], axis=dim)
 
 
 def rms_scale(values_in, eps_value):
@@ -90,7 +103,7 @@
     soft_stats = lax.cond(needed(key_docs, jnp.int32(0)), stats_update, stats_keep, stats_init)
     apply_key_first = lax.all_gather(key_one, "sp", axis=0, tiled=True)
     apply_key_second = lax.all_gather(key_two, "sp", axis=0, tiled=True)
-    value_block = lax.all_gather(values, "sp", axis=0, tiled=True)
+    value_block = collect(values, "sp", 0)
     apply_key_docs = lax.all_gather(documents, "sp", axis=0, tiled=True)
 
     def apply_update(current):

time: 389 us -> 375 us (0.964)
  waiting for transfers between devices: 191 us -> 137 us
  local copies, waits for them, and re-layouts: 32.8 us -> 55.7 us
  starting transfers between devices: 4.67 us -> 22.2 us
    all_gather x1 -> x0, waiting for transfers between devices: 39 us -> none  [local(): value_block = lax.all_gather(values, 'sp', axis=0, tiled=True)]
    all_gather x1, waiting for transfers between devices: 40.5 us -> 6.67 us  [local(): key_second = lax.all_gather(key_two, 'sp', axis=0, tiled=True)]
    ppermute x0 -> x7, waiting for transfers between devices: none -> 26.4 us  [the longest x4 26.4 us: collect(): earlier.append(lax.ppermute(earlier[-1], axis, up))]
    ppermute x0 -> x7, starting transfers between devices: none -> 17.6 us  [the longest x3 9.52 us: collect(): later.append(lax.ppermute(later[-1], axis, down))]
    unnamed x32 -> x47, local copies, waits for them, and re-layouts: 8.52 us -> 25.6 us
    all_gather x1, waiting for transfers between devices: 8.64 us -> 0.01 us  [local(): apply_key_first = lax.all_gather(key_one, 'sp', axis=0, tiled=True)]
    dynamic_slice x0 -> x1, local copies, waits for them, and re-layouts: none -> 4.33 us  [collect(): jnp.roll(line, (lax.axis_index(axis) - ways // 2) * array.shape[dim], axi...]
  transfers between devices with their start and end apart: 6 -> 12, of which waited for: 6 -> 7; matrix products, arithmetic and copies ran while one was open for 6% -> 9% of each run, Pallas kernels for 0% -> 0%
where the time goes in v1:
time: 375 us; the launch traced here: 374 us
  waiting for transfers between devices  137 us (37%)
  blocking collectives  71.7 us (19%)
  local copies, waits for them, and re-layouts  55.7 us (15%)
  matrix products  37.5 us (10%)
  other arithmetic  34.3 us (9%)
  starting transfers between devices  22.2 us (6%)
  between operations  15.2 us (4%)
    all_to_all x1, blocking collectives, local(): lax.all_to_all(outgoing, 'sp', split_axis=0, concat_axis=0, tiled=True)  53.1 us
    all_to_all x1, waiting for transfers between devices, local(): lax.all_to_all(result.reshape(seq_size, item_count, model_width), 'sp', s...  45.3 us
    psum x1, waiting for transfers between devices, local(): lax.psum(proj_term.astype(jnp.bfloat16), 'tp').astype(jnp.float32)  34.7 us
    ppermute x4, waiting for transfers between devices, collect(): earlier.append(lax.ppermute(earlier[-1], axis, up))  26.4 us
    unnamed x47, local copies, waits for them, and re-layouts  25.6 us
    reduce_scatter x1, waiting for transfers between devices, local(): lax.psum_scatter((routed + shared_out).astype(jnp.bfloat16), 'tp', scatte...  23.9 us
    all_gather x1, blocking collectives, local(): apply_key_docs = lax.all_gather(documents, 'sp', axis=0, tiled=True)  18.7 us
    reduce_sum x1, other arithmetic, local(): jnp.sum((picked * picked_weight[:, None]).reshape(tok_rows, route_slots,...  11.4 us
  transfers between devices with their start and end apart: 12, of which 7 were waited for; matrix products, arithmetic and copies ran while one was open for 9% of the time, Pallas kernels for 0%

profile of v1, /device:TPU:0, one launch (start us, length us, event | category | flops | bytes accessed | tf_op | source)
XLA Modules:
  0.0 373.9 jit_solution(313889155098211797)
XLA Ops:
  6.5 1.8 copy.57
  9.5 3.0 collective-permute-start
  12.5 3.1 collective-permute-start.4
  15.6 1.7 copy.59
  18.5 2.3 reduce-window.6
  20.8 4.3 %collective-permute-done = bf16[256,512]{0,1:T(8,128)(2,1)S(1)} collective-permute-done((bf16[256,512]{0,1:T(8,128)(2,1)S(1)}, bf16[256,512]{0,1:T(8,128)(2,1)S(1)}, u32[]{:S(2)}, u32[]{:S(2)}) %collective-permute-start) | collective-permute-done | bytes 262176 | tf_op jit(solution)/shard_map/ppermute | solution.py:16
  25.1 2.5 collective-permute-start.1
  28.1 10.8 %collective-permute-done.1 = bf16[256,512]{0,1:T(8,128)(2,1)S(1)} collective-permute-done((bf16[256,512]{0,1:T(8,128)(2,1)S(1)}, bf16[256,512]{0,1:T(8,128)(2,1)S(1)}, u32[]{:S(2)}, u32[]{:S(2)}) %collective-permute-start.1) | collective-permute-done | bytes 262176 | tf_op jit(solution)/shard_map/ppermute | solution.py:16
  39.5 4.7 %collective-permute-start.5 = (bf16[256,512]{0,1:T(8,128)(2,1)S(1)}, bf16[256,512]{0,1:T(8,128)(2,1)}, u32[]{:S(2)}, u32[]{:S(2)}) collective-permute-start(bf16[256,512]{0,1:T(8,128)(2,1)S(1)} %collective-permute-done.4), channel_id=1, source_target_pairs={{0,28},{4,0},{8,4},{12,8},{16,12},{20,16},{24,20},{28,24},{1,29},{... | collective-permute-start | bytes 786440 | tf_op jit(solution)/shard_map/ppermute | solution.py:18
  44.3 11.3 %collective-permute-done.2 = bf16[256,512]{0,1:T(8,128)(2,1)} collective-permute-done((bf16[256,512]{0,1:T(8,128)(2,1)S(1)}, bf16[256,512]{0,1:T(8,128)(2,1)}, u32[]{:S(2)}, u32[]{:S(2)}) %collective-permute-start.2) | collective-permute-done | bytes 262176 | tf_op jit(solution)/shard_map/ppermute | solution.py:16
  55.6 2.6 collective-permute-start.3
  58.7 1.3 slice.13
  60.5 18.7 %all-gather = s32[8,1,256]{2,1,0:T(1,128)S(1)} all-gather(s32[1,1,256]{2,1,0:T(1,128)} %bitcast.93), channel_id=1, replica_groups=mesh['sp'=8,'tp'=4] {'sp'}, dimensions={0}, use_global_device_ids=true | all-gather | bytes 9216 | tf_op jit(solution)/shard_map/all_gather | solution.py:107
  83.1 1.3 broadcast_add_fusion
  84.4 1.7 collective-permute-start.6
  86.1 1.7 constant_dynamic-update-slice_fusion.15
  87.8 1.7 constant_dynamic-update-slice_fusion.14
  92.5 1.7 constant_dynamic-update-slice_fusion.9
  94.9 1.7 constant_dynamic-update-slice_fusion.7
  96.6 1.7 constant_dynamic-update-slice_fusion.6
  101.3 1.7 constant_dynamic-update-slice_fusion.1
  103.7 6.7 %all-gather.6.cloned.1.call-done = bf16[2048,256]{0,1:T(8,128)(2,1)} async-done(((bf16[256,256]{0,1:T(8,128)(2,1)}), bf16[2048,256]{0,1:T(8,128)(2,1)}) %all-gather.6.cloned.1.call-update) | async-done | bytes 1048592 | tf_op jit(solution)/shard_map/all_gather | solution.py:84
  110.4 13.7 %conditional.2 = (f32[4,256]{1,0:T(4,128)}, f32[4,256]{1,0:T(4,128)}, f32[4,256]{1,0:T(4,128)}, f32[4,256]{1,0:T(4,128)}) conditional(s32[]{:T(128)} %convert_element_type.56, () %tuple.35, (s32[256]{0:T(256)}, s32[2048]{0:T(1024)S(1)}, s32[256]{0:T(256)S(1)}, bf16[2048,256]{0,1:T(8,128)(2,1)}, bf16[256,4,64]{0,2,1:T(8,128)(2,1)S(1)}, ...), branch_computations={%region_1.0_spmd, %region_2.7_spmd} | conditional | flops 571996160 | bytes 50120764 | solution.py:103
  111.6 2.6 fusion.55
  114.2 3.1 fusion.1
  117.9 6.1 %select_reduce_fusion = (f32[4,256]{1,0:T(4,128)}, f32[4,256]{1,0:T(4,128)}) fusion(f32[4,256,2048]{2,1,0:T(8,128)S(1)} %get-tuple-element.293, f32[4,256]{1,0:T(4,128)} %get-tuple-element.309, pred[256,2048]{1,0:T(8,128)(4,1)S(1)} %fusion.2, f32[4,256]{1,0:T(4,128)} %get-tuple-element.307, f32[4,256,2048]{2,1,0:T(8,128)S(1)} %fusion.55), kind=kLoop, calls=%fused_computation.2 | loop fusion | flops 20969472 | bytes 17317888 | tf_op jit(solution)/shard_map/cond/branch_1_fun/reduce_sum | solution.py:97
  124.0 19.7 %conditional.3 = (f32[4,256,128]{1,2,0:T(8,128)}, f32[4,256,1]{1,0,2:T(4,128)S(1)}) conditional(s32[]{:T(128)} %convert_element_type.56, () %tuple.34, (s32[256]{0:T(256)}, s32[2048]{0:T(1024)S(1)}, s32[256]{0:T(256)}, bf16[2048,256]{0,1:T(8,128)(2,1)}, bf16[256,4,64]{0,2,1:T(8,128)(2,1)S(1)}, /*index=5*/f32[4,256]{1,0:T(4,128)}, ...), branch_computations={%region_7.8_spmd, %region_8.10_spmd.clone} | conditional | flops 1098644480 | bytes 31234324 | solution.py:129
  124.0 4.3 %constant_dynamic-slice_fusion = bf16[2048,512]{0,1:T(8,128)(2,1)} fusion(bf16[4096,512]{0,1:T(8,128)(2,1)} %get-tuple-element.240, s32[]{:T(128)S(6)} %select_n.172), kind=kLoop, calls=%fused_computation.22 | loop fusion | bytes 4194308 | tf_op jit(solution)/shard_map/jit(_roll_dynamic)/dynamic_slice | solution.py:20
  128.4 4.5 %fusion.56 = f32[4,256,2048]{2,1,0:T(8,128)} fusion(bf16[256,4,64]{0,2,1:T(8,128)(2,1)S(1)} %get-tuple-element.232, bf16[2048,4,64]{0,2,1:T(8,128)(2,1)S(1)} %bitcast.75), kind=kOutput, calls=%fused_computation.130 | convolution fusion | flops 268435456 | bytes 9568256 | tf_op jit(solution)/shard_map/cond/branch_1_fun/qhd,khd->hqk/dot_general | solution.py:75
  133.4 10.3 %multiply_reduce_fusion = (f32[4,256]{1,0:T(4,128)S(1)}, f32[4,256,128]{1,2,0:T(8,128)}) fusion(bf16[2048,4,128]{0,2,1:T(8,128)(2,1)} %bitcast.77, f32[4,256,2048]{2,1,0:T(8,128)} %fusion.56, bf16[256,4,64]{0,2,1:T(8,128)(2,1)S(1)} %get-tuple-element.236, bf16[2048,4,64]{0,2,1:T(8,128)(2,1)} %bitcast.83, f32[4,256]{1,0:T(4,128)} %get-tuple-element.239, ...), kind=kOutput, calls=%fused_computation.21 | convolution fusion | flops 828636160 | bytes 12734480 | tf_op jit(solution)/shard_map/cond/branch_1_fun/hqk,khv->hqv/dot_general | solution.py:122
  145.0 3.4 convolution_convert_fusion.1
  149.1 34.7 %all-reduce.2.cloned.1.call-done = bf16[256,2048]{1,0:T(8,128)(2,1)} async-done(((bf16[256,2048]{1,0:T(8,128)(2,1)}), bf16[256,2048]{1,0:T(8,128)(2,1)}) %all-reduce.2.cloned.1.call-update) | async-done | bytes 1048592 | tf_op jit(solution)/shard_map/psum | solution.py:137
  183.9 3.0 convert_add_fusion
  187.5 3.3 gather_fusion
  190.8 1.9 broadcast_select_fusion
  192.8 53.1 %all_to_all.10 = bf16[8,64,2048]{2,1,0:T(8,128)(2,1)S(1)} all-to-all(bf16[8,64,2048]{2,1,0:T(8,128)(2,1)S(1)} %broadcast_select_fusion), channel_id=1, replica_groups=mesh['sp'=8,'tp'=4] {'sp'}, dimensions={0} | all-to-all | bytes 4194304 | tf_op jit(solution)/shard_map/all_to_all | solution.py:161
  245.8 1.3 copy-done.5
  247.2 2.2 fusion.16
  249.4 6.3 %convolution_convert_fusion = bf16[512,2048]{1,0:T(8,128)(2,1)} fusion(bf16[1,512,2048]{2,1,0:T(8,128)(2,1)S(1)} %copy-done, bf16[512,2048]{1,0:T(8,128)(2,1)} %bitcast.79, bf16[1,2048,512]{2,1,0:T(8,128)(2,1)} %param.37, f32[512,512]{1,0:T(8,128)} %fusion.16), kind=kOutput, calls=%fused_computation.26 | convolution fusion | flops 2150105088 | bytes 9437184 | tf_op jit(solution)/shard_map/dot_general | solution.py:167
  255.7 4.5 %all-to-all-start.1 = ((bf16[8,64,2048]{2,1,0:T(8,128)(2,1)}), bf16[8,64,2048]{2,1,0:T(8,128)(2,1)}, u32[]{:S(2)}, u32[]{:S(2)}) async-start(bf16[8,64,2048]{2,1,0:T(8,128)(2,1)} %bitcast.76), calls=%async_computation.1 | async-start | bytes 4194304 | tf_op jit(solution)/shard_map/all_to_all | solution.py:170
  260.6 1.5 fusion.57
  262.1 45.3 %all-to-all-done.1 = bf16[8,64,2048]{2,1,0:T(8,128)(2,1)} async-done(((bf16[8,64,2048]{2,1,0:T(8,128)(2,1)}), bf16[8,64,2048]{2,1,0:T(8,128)(2,1)}, u32[]{:S(2)}, u32[]{:S(2)}) %all-to-all-start.1) | async-done | bytes 2097184 | tf_op jit(solution)/shard_map/all_to_all | solution.py:170
  307.4 10.7 %gather_fusion.1 = bf16[1024,2048]{1,0:T(8,128)(2,1)} fusion(bf16[512,2048]{1,0:T(8,128)(2,1)} %bitcast.20, s32[1024]{0:T(1024)S(1)} %broadcast_clamp_fusion), kind=kCustom, calls=%fused_computation.1 | custom fusion | bytes 8392704 | tf_op jit(solution)/shard_map/gather | solution.py:178
  318.1 8.3 %reshape.457 = f32[256,4,2048]{2,1,0:T(4,128)} reshape(bf16[1024,2048]{1,0:T(8,128)(2,1)} %gather_fusion.1) | data formatting | bytes 12582912 | tf_op jit(solution)/shard_map/convert_element_type | solution.py:178
  326.4 11.4 %multiply_reduce_fusion.1 = f32[256,2048]{1,0:T(8,128)} fusion(f32[256,4,2048]{2,1,0:T(4,128)} %reshape.457, f32[256,4]{1,0:T(8,128)S(1)} %copy.68), kind=kLoop, calls=%fused_computation.25 | loop fusion | flops 3670016 | bytes 10489856 | tf_op jit(solution)/shard_map/reduce_sum | solution.py:180
  337.8 3.7 fusion.12
  341.6 23.9 %reduce-scatter.2.cloned.1.call-done = bf16[64,2048]{1,0:T(8,128)(2,1)} async-done(((bf16[256,2048]{1,0:T(8,128)(2,1)}), bf16[64,2048]{1,0:T(8,128)(2,1)}) %reduce-scatter.2.cloned.1.call-update) | async-done | bytes 262160 | tf_op jit(solution)/shard_map/reduce_scatter | solution.py:188
  365.5 1.9 add_convert_fusion
  (92 shorter events, 19.4 us)
Async XLA Ops:
  6.5 242.9 %copy-start = (bf16[1,512,2048]{2,1,0:T(8,128)(2,1)S(1)}, bf16[1,512,2048]{2,1,0:T(8,128)(2,1)}, u32[]{:S(2)}) copy-start(bf16[1,512,2048]{2,1,0:T(8,128)(2,1)} %param.38) | copy-start | bytes 6291460
  6.5 97.1 %all-gather.4.cloned.1.call-start = ((), (), s32[]{:S(2)}) async-start(), calls=%async_computation.3 | async-start | bytes 1179648 | tf_op jit(solution)/shard_map/all_gather | solution.py:104
  8.4 102.0 %all-gather.6.cloned.1.call-start = ((), (), s32[]{:S(2)}) async-start(), calls=%async_computation.4 | async-start | bytes 1179648 | tf_op jit(solution)/shard_map/all_gather | solution.py:84
  9.5 15.6 %collective-permute-start = (bf16[256,512]{0,1:T(8,128)(2,1)S(1)}, bf16[256,512]{0,1:T(8,128)(2,1)S(1)}, u32[]{:S(2)}, u32[]{:S(2)}) collective-permute-start(bf16[256,512]{0,1:T(8,128)(2,1)S(1)} %copy.61), channel_id=1, source_target_pairs={{0,4},{4,8},{8,12},{12,16},{16,20},{20,24},{24,28},{28,0},{1,5},{5... | collective-permute-start | bytes 786440 | tf_op jit(solution)/shard_map/ppermute | solution.py:16
  12.5 27.0 %collective-permute-start.4 = (bf16[256,512]{0,1:T(8,128)(2,1)S(1)}, bf16[256,512]{0,1:T(8,128)(2,1)S(1)}, u32[]{:S(2)}, u32[]{:S(2)}) collective-permute-start(bf16[256,512]{0,1:T(8,128)(2,1)S(1)} %copy.61), channel_id=1, source_target_pairs={{0,28},{4,0},{8,4},{12,8},{16,12},{20,16},{24,20},{28,24},{1,29},{... | collective-permute-start | bytes 786440 | tf_op jit(solution)/shard_map/ppermute | solution.py:18
  17.3 166.5 %all-reduce.2.cloned.1.call-start = ((), (), s32[]{:S(2)}) async-start(), calls=%async_computation.5 | async-start | bytes 2097152 | tf_op jit(solution)/shard_map/psum | solution.py:137
  25.1 13.8 %collective-permute-start.1 = (bf16[256,512]{0,1:T(8,128)(2,1)S(1)}, bf16[256,512]{0,1:T(8,128)(2,1)S(1)}, u32[]{:S(2)}, u32[]{:S(2)}) collective-permute-start(bf16[256,512]{0,1:T(8,128)(2,1)S(1)} %collective-permute-done), channel_id=1, source_target_pairs={{0,4},{4,8},{8,12},{12,16},{16,20},{20,24},{24,28},{28,0},{1,5},{5... | collective-permute-start | bytes 786440 | tf_op jit(solution)/shard_map/ppermute | solution.py:16
  38.9 16.7 %collective-permute-start.2 = (bf16[256,512]{0,1:T(8,128)(2,1)S(1)}, bf16[256,512]{0,1:T(8,128)(2,1)}, u32[]{:S(2)}, u32[]{:S(2)}) collective-permute-start(bf16[256,512]{0,1:T(8,128)(2,1)S(1)} %collective-permute-done.1), channel_id=1, source_target_pairs={{0,4},{4,8},{8,12},{12,16},{16,20},{20,24},{24,28},{28,0},{1,5},{5... | collective-permute-start | bytes 786440 | tf_op jit(solution)/shard_map/ppermute | solution.py:16
  39.5 44.9 %collective-permute-start.5 = (bf16[256,512]{0,1:T(8,128)(2,1)S(1)}, bf16[256,512]{0,1:T(8,128)(2,1)}, u32[]{:S(2)}, u32[]{:S(2)}) collective-permute-start(bf16[256,512]{0,1:T(8,128)(2,1)S(1)} %collective-permute-done.4), channel_id=1, source_target_pairs={{0,28},{4,0},{8,4},{12,8},{16,12},{20,16},{24,20},{28,24},{1,29},{... | collective-permute-start | bytes 786440 | tf_op jit(solution)/shard_map/ppermute | solution.py:18
  55.6 30.5 %collective-permute-start.3 = (bf16[256,512]{0,1:T(8,128)(2,1)}, bf16[256,512]{0,1:T(8,128)(2,1)}, u32[]{:S(2)}, u32[]{:S(2)}) collective-permute-start(bf16[256,512]{0,1:T(8,128)(2,1)} %collective-permute-done.2), channel_id=1, source_target_pairs={{0,4},{4,8},{8,12},{12,16},{16,20},{20,24},{24,28},{28,0},{1,5},{5... | collective-permute-start | bytes 786440 | tf_op jit(solution)/shard_map/ppermute | solution.py:16
  58.2 22.9 %copy-start.13 = (s32[256]{0:T(256)}, s32[256]{0:T(256)S(1)}, u32[]{:S(2)}) copy-start(s32[256]{0:T(256)S(1)} %iota_add_fusion) | copy-start | bytes 3076
  84.4 25.9 %copy-start.10 = (s32[256]{0:T(256)S(1)}, s32[256]{0:T(256)}, u32[]{:S(2)}) copy-start(s32[256]{0:T(256)} %param.29) | copy-start | bytes 3076
  84.4 9.7 %collective-permute-start.6 = (bf16[256,512]{0,1:T(8,128)(2,1)}, bf16[256,512]{0,1:T(8,128)(2,1)S(1)}, u32[]{:S(2)}, u32[]{:S(2)}) collective-permute-start(bf16[256,512]{0,1:T(8,128)(2,1)} %collective-permute-done.5), channel_id=1, source_target_pairs={{0,28},{4,0},{8,4},{12,8},{16,12},{20,16},{24,20},{28,24},{1,29},{... | collective-permute-start | bytes 786440 | tf_op jit(solution)/shard_map/ppermute | solution.py:18
  111.6 2.6 copy-start.6
  124.0 4.3 %copy-start.1 = (bf16[2048,256]{0,1:T(8,128)(2,1)S(1)}, bf16[2048,256]{0,1:T(8,128)(2,1)}, u32[]{:S(2)}) copy-start(bf16[2048,256]{0,1:T(8,128)(2,1)} %get-tuple-element.233) | copy-start | bytes 3145732 | tf_op jit(solution)/shard_map/cond
  128.4 4.5 %copy-start.11 = (s32[256]{0:T(256)S(1)}, s32[256]{0:T(256)}, u32[]{:S(2)}) copy-start(s32[256]{0:T(256)} %get-tuple-element.231) | copy-start | bytes 3076 | tf_op jit(solution)/shard_map/cond
  128.4 4.5 %copy-start.14 = (s32[256]{0:T(256)S(1)}, s32[256]{0:T(256)}, u32[]{:S(2)}) copy-start(s32[256]{0:T(256)} %get-tuple-element.229) | copy-start | bytes 3076 | tf_op jit(solution)/shard_map/cond
  143.7 5.1 %copy-start.9 = (s32[1024]{0:T(1024)S(1)}, s32[1024]{0:T(1024)}, u32[]{:S(2)}) copy-start(s32[1024]{0:T(1024)} %get-tuple-element.302) | copy-start | bytes 12292
  143.7 40.1 %copy-start.2 = (bf16[256,2048]{1,0:T(8,128)(2,1)S(1)}, bf16[256,2048]{1,0:T(8,128)(2,1)}, u32[]{:S(2)}) copy-start(bf16[256,2048]{1,0:T(8,128)(2,1)} %param.23) | copy-start | bytes 3145732
  145.0 41.9 %copy-start.12 = (f32[2048]{0:T(1024)S(1)}, f32[2048]{0:T(1024)}, u32[]{:S(2)}) copy-start(f32[2048]{0:T(1024)} %param.33) | copy-start | bytes 24580
  183.8 3.1 copy-start.3
  183.8 3.1 copy-start.4
  190.8 56.3 %copy-start.16 = (bf16[1,2048,512]{2,1,0:T(8,128)(2,1)S(1)}, bf16[1,2048,512]{2,1,0:T(8,128)(2,1)}, u32[]{:S(2)}) copy-start(bf16[1,2048,512]{2,1,0:T(8,128)(2,1)} %param.36) | copy-start | bytes 6291460
  245.8 1.3 copy-start.5
  255.7 4.7 %copy-start.7 = (s32[256,4]{0,1:T(4,128)S(1)}, s32[256,4]{0,1:T(4,128)}, u32[]{:S(2)}) copy-start(s32[256,4]{0,1:T(4,128)} %param.34) | copy-start | bytes 12292
  255.7 4.7 %copy-start.15 = (f32[256,4]{0,1:T(4,128)S(1)}, f32[256,4]{0,1:T(4,128)}, u32[]{:S(2)}) copy-start(f32[256,4]{0,1:T(4,128)} %param.35) | copy-start | bytes 12292
  255.7 4.9 %copy-start.8 = (s32[1024]{0:T(1024)S(1)}, s32[1024]{0:T(1024)}, u32[]{:S(2)}) copy-start(s32[1024]{0:T(1024)} %get-tuple-element.300) | copy-start | bytes 12292
  255.7 51.8 %all-to-all-start.1 = ((bf16[8,64,2048]{2,1,0:T(8,128)(2,1)}), bf16[8,64,2048]{2,1,0:T(8,128)(2,1)}, u32[]{:S(2)}, u32[]{:S(2)}) async-start(bf16[8,64,2048]{2,1,0:T(8,128)(2,1)} %bitcast.76), calls=%async_computation.1 | async-start | bytes 4194304 | tf_op jit(solution)/shard_map/all_to_all | solution.py:170
  260.2 105.3 %reduce-scatter.2.cloned.1.call-start = ((), (), s32[]{:S(2)}) async-start(), calls=%async_computation.6 | async-start | bytes 1310720 | tf_op jit(solution)/shard_map/reduce_scatter | solution.py:188
Sparse Core Ops, SparseCore 0:
  9.4 56.0 all-gather.3
  67.5 42.8 all-gather.5
  148.5 35.2 all-reduce.1
  341.7 23.7 reduce-scatter.1
